TPU v7x, 32 devices: a whole 2x2x4 slice. The times are simulated.
32 devices in a mesh: sp: 16 (over z, y, x), tp: 2 (over core).
Axes of the slice: x: 2, y: 2, z: 4, core: 2. Of those that a mesh axis runs over, the one named last changes fastest.
Arguments:
- resid: bfloat16 [6144, 2048], P(('sp', 'tp')), may hold values from -6 to 6
- q_small: bfloat16 [6144, 1024], P('sp', 'tp'), may hold values from -6 to 6
- k_small: bfloat16 [6144, 1024], P('sp', 'tp'), may hold values from -6 to 6
- v_small: bfloat16 [6144, 1024], P('sp', 'tp'), may hold values from -6 to 6
- q_large: bfloat16 [6144, 1024], P('sp', 'tp'), may hold values from -6 to 6
- k_large: bfloat16 [6144, 1024], P('sp', 'tp'), may hold values from -6 to 6
- v_large: bfloat16 [6144, 1024], P('sp', 'tp'), may hold values from -6 to 6
- gate_small: bfloat16 [6144, 1024], P('sp', 'tp'), may hold values from -6 to 6
- large_head_gate: bfloat16 [6144, 1024], P('sp', 'tp'), may hold values from -6 to 6
- gates_small: float32 [6144, 3, 16], P('sp', None, 'tp'), may hold values from -6 to 300, as said below
- gates_large: float32 [6144, 3, 8], P('sp', None, 'tp'), may hold values from -6 to 300, as said below
- w_out_small: bfloat16 [1024, 2048], P('tp'), may hold values from -0.125 to 0.125
- w_out_large: bfloat16 [1024, 2048], P('tp'), may hold values from -0.125 to 0.125
- norm_gain: float32 [2048], replicated, may hold values from 0.1 to 1.9
- expert_ids: int32 [6144, 2], P(('sp', 'tp')), may hold values from 0 to 15, all different within a row; in each aligned block of 192 rows (0 to 191, 192 to 383, ...) at most 48 rows name the same one
- expert_weight: float32 [6144, 2], P(('sp', 'tp')), may hold values from 0.2 to 1
- w_gate: bfloat16 [16, 2048, 2048], P('sp', None, 'tp'), may hold values from -0.125 to 0.125
- w_up: bfloat16 [16, 2048, 2048], P('sp', None, 'tp'), may hold values from -0.125 to 0.125
- w_down: bfloat16 [16, 2048, 2048], P('sp', 'tp'), may hold values from -0.125 to 0.125
Outputs:
- layer_out: bfloat16 [6144, 2048], P(('sp', 'tp'))
Inputs may be any that keep to these rules, and one draw needn't show every extreme that they name: `gates_small`: field 0 is the input gate's pre-activation, field 1 the forget gate's pre-activation, field 2 a non-positive term added to the log forget gate. `gates_large`: field 0 is the input gate's pre-activation, field 1 the forget gate's pre-activation, field 2 a non-positive term added to the log forget gate. `expert_ids`: each row names 2 different experts. In the 192 rows of one device no expert is named by more than 48 rows, and in some device's rows an expert is named exactly 48 times.
All inputs are finite; a program needn't handle non-finite values.
Results may differ from a plain program's by a relative error of at most 0.014.
Values may be sent and summed in bfloat16 or wider, within the bound.
A program may use at most 128 MiB of HBM per device.

v0:
```python
import functools

import jax
import jax.numpy as jnp
from jax import lax
from jax.experimental import pallas as pl
from jax.experimental.pallas import tpu as pltpu
from jax.sharding import PartitionSpec as P

floor_neg = -1e30
norm_eps = 1e-06
LANES = 128
MESH = pl.DeviceIdType.MESH
F32 = jnp.float32
BF16 = jnp.bfloat16


def iota(shape, axis):
    return lax.broadcasted_iota(jnp.int32, shape, axis)


def dot(a, b, ca=1, cb=0, **kw):
    return lax.dot_general(
        a, b, (((ca,), (cb,)), ((), ())), preferred_element_type=F32, **kw
    )


def exact_dot(a, b):
    return dot(a, b, precision=lax.Precision.HIGHEST)


def mixer_part(
    dims, opened,
    gates, ks, vs, kl, vl, qs, ql, gs_far, gl_far, ws_far, wl_far, resid_far, gain,
    after_ref, out_ref, ws, wl, resid, psend, precv, y,
    gs, gl,
    tot_c, tot_a, give_c, got_c, got_a, sum_c, sum_a, past_c, past_a, lead_c, pre_c, pre_a,
    inum, imax, iden,
    lsem, s1, r1, s2, r2, s2a, r2a, s3, r3, psem, rsem,
):
    planes, heads_s, heads_l = dims
    length = qs.shape[0]
    per = heads_s * LANES // qs.shape[1]
    half = LANES // per
    pairs = heads_s // per
    units = pairs + heads_l
    rows = length // 2
    me = lax.axis_index("sp")
    core = lax.axis_index("tp")
    other = 1 - core
    size = lax.axis_size("sp") // planes
    z, mine = me // size, lax.rem(me, size)
    slice_rows = tot_c.shape[0] // size

    loads = [
        pltpu.make_async_copy(src, dst, lsem.at[i])
        for i, (src, dst) in enumerate(
            ((gs_far, gs), (gl_far, gl), (ws_far, ws), (wl_far, wl), (resid_far, resid))
        )
    ]
    for load in loads:
        load.start()

    sides = [lax.rem(mine + i, size) for i in range(1, size)]
    others = [lax.rem(z + i, planes) for i in range(1, planes)]
    barrier = pltpu.get_barrier_semaphore()
    for to in [z * size + p for p in sides] + [d * size + mine for d in others]:
        pl.semaphore_signal(barrier, inc=1, device_id={"sp": to}, device_id_type=MESH)
    pl.semaphore_signal(barrier, inc=1, device_id={"tp": other}, device_id_type=MESH)

    def remote(src, dst, ssem, rsem, to):
        return pltpu.make_async_remote_copy(
            src, dst, ssem, rsem, device_id={"sp": to}, device_id_type=MESH
        )

    lane = iota((1, LANES), 1)

    def spread(columns):
        if len(columns) == 1:
            return jnp.broadcast_to(columns[0], (columns[0].shape[0], LANES))
        picked = columns[0]
        for i in range(1, len(columns)):
            picked = jnp.where(lane >= i * half, columns[i], picked)
        return picked

    def heads_of(unit):
        if unit < pairs:
            return list(range(unit * per, (unit + 1) * per))
        return [heads_s + unit - pairs]

    def view(small, large, unit):
        if unit < pairs:
            return small[:, unit * LANES : (unit + 1) * LANES]
        low = (unit - pairs) * LANES
        return large[:, low : low + LANES]

    def span(unit):
        if unit < pairs:
            return unit * half, half
        return pairs * half + (unit - pairs) * LANES, LANES

    upper_tri = (iota((length, length), 0) <= iota((length, length), 1)).astype(F32)
    lit = gates[0]
    lft = jax.nn.log_sigmoid(gates[1]) + gates[2]
    cum_row = exact_dot(lft, upper_tri)
    u_row = lit - cum_row
    cum_col = cum_row.T
    total = cum_col[length - 1 : length, :]
    grow = total - cum_col + lit.T
    peak = jnp.max(grow, axis=0, keepdims=True)
    factor = jnp.exp(grow - peak)

    for unit in range(units):
        hs = heads_of(unit)
        key = view(ks, kl, unit).astype(F32)
        scaled = spread([factor[:, h : h + 1] for h in hs]) * key
        full = dot(scaled.astype(BF16), view(vs, vl, unit), 0, 0)
        low, extent = span(unit)
        if unit < pairs:
            packed = full[:half]
            for i in range(1, per):
                packed = jnp.where(lane >= i * half, full[i * half : (i + 1) * half], packed)
        else:
            packed = full
        tot_c[low : low + extent, :] = packed
        tot_a[unit : unit + 1, :] = jnp.sum(scaled, axis=0, keepdims=True)
        tot_a[units + unit : units + unit + 1, :] = spread([peak[:, h : h + 1] for h in hs])
        tot_a[2 * units + unit : 2 * units + unit + 1, :] = spread(
            [total[:, h : h + 1] for h in hs]
        )

    def join(early, late):
        em, eb = early[units : 2 * units], early[2 * units :]
        lm, lb = late[units : 2 * units], late[2 * units :]
        m = jnp.maximum(em + lb, lm)
        ew, lw = jnp.exp(em + lb - m), jnp.exp(lm - m)
        n = ew * early[:units] + lw * late[:units]
        return jnp.concatenate([n, m, eb + lb], axis=0), ew, lw

    def owned(p):
        return pl.ds(pl.multiple_of(p * slice_rows, 16), slice_rows)

    place = iota((slice_rows, units), 0) + mine * slice_rows
    unit_at = iota((slice_rows, units), 1)
    low_at = jnp.where(unit_at < pairs, unit_at * half, pairs * half + (unit_at - pairs) * LANES)
    high_at = low_at + jnp.where(unit_at < pairs, half, LANES)
    holds = ((place >= low_at) & (place < high_at)).astype(F32)

    def widen(weights):
        wide = exact_dot(holds, jnp.concatenate(weights, axis=1))
        return [wide[:, i * LANES : (i + 1) * LANES] for i in range(len(weights))]

    give_c[...] = tot_c[...].astype(BF16)
    got_c[mine] = give_c[owned(mine), :]
    got_a[mine] = tot_a[...]
    none_a = jnp.concatenate(
        [
            jnp.zeros((units, LANES), F32),
            jnp.full((units, LANES), floor_neg, F32),
            jnp.zeros((units, LANES), F32),
        ],
        axis=0,
    )
    for d in range(planes):

        @pl.when(z <= d)
        def _():
            past_c[d] = jnp.zeros_like(past_c[d])
            past_a[d] = none_a

    def first(p):
        to = z * size + p
        return (
            remote(give_c.at[owned(p)], got_c.at[mine], s1.at[0], r1.at[0], to),
            remote(tot_a, got_a.at[mine], s1.at[1], r1.at[1], to),
        )

    def second(d):
        to = d * size + mine
        return (
            remote(sum_c, past_c.at[z], s2.at[d], r2.at[z], to),
            remote(sum_a, past_a.at[z], s2a.at[d], r2a.at[z], to),
        )

    def reached(d):
        return (
            remote(sum_c, past_c.at[d], s2.at[d], r2.at[d], me),
            remote(sum_a, past_a.at[d], s2a.at[d], r2a.at[d], me),
        )

    def third(j):
        return remote(
            lead_c.at[j], pre_c.at[owned(mine)], s3.at[0], r3.at[0], z * size + j
        )

    crowd = pl.ds(0, size - 1)
    firsts = (
        remote(got_c.at[crowd], got_c.at[crowd], s1.at[0], r1.at[0], me),
        remote(got_a.at[crowd], got_a.at[crowd], s1.at[1], r1.at[1], me),
    )
    thirds = remote(lead_c.at[crowd], lead_c.at[crowd], s3.at[0], r3.at[0], me)

    block = LANES

    def inner(unit):
        hs = heads_of(unit)
        scale = (half if unit < pairs else LANES) ** (-0.5)
        q, k, v = view(qs, ql, unit), view(ks, kl, unit), view(vs, vl, unit)
        for start in range(0, length, block):
            width = start + block
            causal = iota((block, width), 1) <= iota((block, width), 0) + start
            nums, tops, dens = [], [], []
            for i, h in enumerate(hs):
                q_block = q[start : start + block]
                if len(hs) > 1:
                    mine = (lane >= i * half) & (lane < (i + 1) * half)
                    q_block = jnp.where(mine, q_block, jnp.zeros_like(q_block))
                raw = dot(q_block, k[:width], 1, 1) * scale
                masked = jnp.where(causal, u_row[h : h + 1, :width], floor_neg)
                top = jnp.max(masked, axis=1, keepdims=True)
                scored = raw * jnp.exp(masked - top)
                dens.append(jnp.sum(scored, axis=1, keepdims=True))
                tops.append(top)
                nums.append(dot(scored.astype(BF16), v[:width]))
            num = nums[0]
            for i in range(1, len(hs)):
                num = jnp.where(lane >= i * half, nums[i], num)
            inum[unit, start : start + block, :] = num
            imax[unit, start : start + block, :] = spread(tops)
            iden[unit, start : start + block, :] = spread(dens)

    pl.semaphore_wait(barrier, len(sides) + len(others) + 1)
    for p in sides:
        for copy in first(p):
            copy.start()
    opened()
    for unit in range(pairs):
        inner(unit)
    for copy in firsts:
        copy.wait_recv()
    blocks = [got_a[i] for i in range(size)]
    whole, weights = blocks[0], [jnp.ones((units, LANES), F32)]
    for i in range(1, size):
        whole, ew, lw = join(whole, blocks[i])
        weights = [w * ew for w in weights] + [lw]
    total_c = 0.0
    for i, w in enumerate(widen(weights)):
        total_c = total_c + w * got_c[i].astype(F32)
    sum_c[...] = total_c.astype(BF16)
    sum_a[...] = whole
    for d in range(planes):

        @pl.when(d > z)
        def _():
            for copy in second(d):
                copy.start()

    for unit in range(pairs, units):
        inner(unit)
    for d in range(planes):

        @pl.when(d < z)
        def _():
            for copy in reached(d):
                copy.wait_recv()

    lead_a, weights = none_a, []
    for d in range(planes):
        lead_a, ew, lw = join(lead_a, past_a[d])
        weights = [w * ew for w in weights] + [lw]
    leads, steps = [lead_a], []
    for j in range(size - 1):
        lead_a, ew, lw = join(lead_a, blocks[j])
        leads.append(lead_a)
        steps += [ew, lw]
    wide = widen(weights + steps)
    state_c = 0.0
    for d in range(planes):
        state_c = state_c + wide[d] * past_c[d].astype(F32)
    for j in range(size):
        lead_c[j] = state_c.astype(BF16)

        @pl.when(j != mine)
        def _():
            third(j).start()

        @pl.when(j == mine)
        def _():
            pre_c[owned(mine), :] = lead_c[j]
            pre_a[...] = leads[j]

        if j < size - 1:
            ew, lw = wide[planes + 2 * j : planes + 2 * j + 2]
            state_c = ew * state_c + lw * got_c[j].astype(F32)
    for load in loads:
        load.wait()
    thirds.wait_recv()

    for unit in range(units):
        hs = heads_of(unit)
        scale = (half if unit < pairs else LANES) ** (-0.5)
        low, extent = span(unit)
        q = view(qs, ql, unit)
        state = pre_c[low : low + extent, :]
        if unit < pairs:
            state = jnp.concatenate(
                [
                    jnp.where((lane >= i * half) & (lane < (i + 1) * half), state, jnp.zeros_like(state))
                    for i in range(per)
                ],
                axis=0,
            )
        inter = dot(q, state) * scale
        qn = q.astype(F32) * pre_a[unit : unit + 1, :]
        if len(hs) > 1:
            parts = [
                jnp.sum(
                    jnp.where((lane >= i * half) & (lane < (i + 1) * half), qn, 0.0),
                    axis=1,
                    keepdims=True,
                )
                for i in range(per)
            ]
        else:
            parts = [jnp.sum(qn, axis=1, keepdims=True)]
        inter_den = spread(parts) * scale
        carry_m = pre_a[units + unit : units + unit + 1, :]
        top = jnp.maximum(carry_m, imax[unit])
        own_w, carry_w = jnp.exp(imax[unit] - top), jnp.exp(carry_m - top)
        numer = own_w * inum[unit] + carry_w * inter
        denom = own_w * iden[unit] + carry_w * inter_den
        memory = numer / jnp.maximum(jnp.abs(denom), 1.0)
        gate = jax.nn.sigmoid(view(gs, gl, unit).astype(F32))
        gated = (gate * memory).astype(BF16)
        for i in range(2):
            at = i * units * LANES + unit * LANES
            y[:, at : at + LANES] = gated[i * rows : (i + 1) * rows]

    cut = qs.shape[1]
    features = ws.shape[1]
    step_n = 512

    def project(which, n):
        low = pl.multiple_of(which * (units * LANES), LANES)
        left = y[:, pl.ds(low, cut)]
        right = y[:, pl.ds(low + cut, units * LANES - cut)]
        at = (slice(None), slice(n, n + step_n))
        return (dot(left, ws[at]) + dot(right, wl[at])).astype(BF16)

    def swap(n):
        at = (slice(None), pl.ds(n, step_n))
        i = n // step_n
        return pltpu.make_async_remote_copy(
            psend.at[at], precv.at[at], psem.at[i], rsem.at[i],
            device_id={"tp": other}, device_id_type=MESH,
        )

    for n in range(0, features, step_n):
        psend[:, n : n + step_n] = project(other, n)
        swap(n).start()
    power = 0.0
    for n in range(0, features, step_n):
        at = (slice(None), slice(n, n + step_n))
        own = project(core, n).astype(F32)
        swap(n).wait_recv()
        after = resid[at].astype(F32) + (own + precv[at].astype(F32))
        after_ref[at] = after
        power = power + jnp.sum(after * after, axis=-1, keepdims=True)
    scale = lax.rsqrt(power * (1.0 / features) + norm_eps)
    for n in range(0, features, step_n):
        at = (slice(None), slice(n, n + step_n))
        out_ref[at] = (after_ref[at] * scale * gain[:, n : n + step_n]).astype(BF16)

    for copy in firsts:
        copy.wait_send()
    for d in range(planes):

        @pl.when(d > z)
        def _():
            for copy in second(d):
                copy.wait_send()

    thirds.wait_send()
    for n in range(0, features, step_n):
        swap(n).wait_send()


def orders(planes):
    centre = (planes - 1) / 2

    def order(z):
        rank = lambda d: (abs(d - z), 0 if (d > z) == (z < centre) else 1)
        return sorted(range(planes), key=rank)

    return [order(z) for z in range(planes)]


def schedule(planes):
    none = -1
    order = orders(planes)
    last = planes + 1
    names = ("work", "next", "also", "mid", "join", "late", "tail")
    rows = {name: [] for name in names}
    for z in range(planes):
        o = order[z]
        plan = [dict.fromkeys(rows, none) for _ in range(last + 1)]
        plan[0].update(next=o[1])
        if z in (0, planes - 1):
            plan[1].update(work=o[1], mid=o[2], join=o[1])
            plan[2].update(work=o[2], mid=o[3], join=o[2])
            plan[3].update(work=o[3], join=o[3])
            plan[4].update(work=o[0])
            plan[5].update(late=o[0])
        else:
            plan[0].update(also=o[2])
            plan[1].update(work=o[1], mid=o[3])
            plan[2].update(work=o[2])
            plan[3].update(work=o[3])
            plan[4].update(work=o[0], join=o[1])
            plan[5].update(join=o[3], tail=o[2], late=o[0])
        for name in rows:
            rows[name].append([step[name] for step in plan])
    return rows, last + 1


def experts_part(
    capacity, planes, loaded, normed, ids, wts, out_ref,
    wg, wu, wd, acc, disp, psend, hidden, ret,
    all_ids, all_wts, sel, comb, tok, arr, pin,
    ids_s, ids_r, wts_s, wts_r, tok_s, tok_r, dis_s, dis_r, ret_s, ret_r, pin_s, pin_r,
):
    peers = lax.axis_size("sp")
    me = lax.axis_index("sp")
    size = peers // planes
    z, mine = me // size, lax.rem(me, size)
    part, features = wd.shape[0] // 2, wd.shape[1]
    rows = normed.shape[0]
    slots = size * capacity
    tile = 512
    chunks = features // tile

    def remote(src, dst, ssem, rsem, to):
        return pltpu.make_async_remote_copy(
            src, dst, ssem, rsem, device_id={"sp": to}, device_id_type=MESH
        )

    def sent(ref, sem):
        return remote(ref, ref, sem, sem, me)

    sides = [lax.rem(mine + i, size) for i in range(1, size)]
    others = [lax.rem(z + i, planes) for i in range(1, planes)]

    def row(d):
        return pl.ds(pl.multiple_of(d * rows, 16), rows)

    def slot(d, p=0, count=slots):
        return pl.ds(pl.multiple_of(d * slots + p * capacity, 16), count)

    def cols(c):
        if isinstance(c, int):
            return pl.ds(c * tile, tile)
        return pl.ds(pl.multiple_of(c * tile, tile), tile)

    def block(p):
        return pl.ds(pl.multiple_of(p * capacity, 16), capacity)

    def tell(d, at):
        to = d * size + mine
        return (
            remote(ids, all_ids.at[at], ids_s.at[d], ids_r.at[at], to),
            remote(wts, all_wts.at[at], wts_s.at[d], wts_r.at[at], to),
        )

    def own_up(c):
        return remote(
            normed.at[:, cols(c)], tok.at[z, :, cols(c)], tok_s.at[z], tok_r.at[z, c],
            me + size,
        )

    def own_down(c):
        return remote(
            normed.at[:, cols(c)], tok.at[z, :, cols(c)], tok_s.at[planes], tok_r.at[z, c],
            me - size,
        )

    def relay(d, c, to):
        return remote(
            tok.at[d, :, cols(c)], tok.at[d, :, cols(c)], tok_s.at[d], tok_r.at[d, c], to
        )

    for d in others:
        for copy in tell(d, z):
            copy.start()
    for c in range(chunks):

        @pl.when(z < planes - 1)
        def _():
            own_up(c).start()

        @pl.when(z > 0)
        def _():
            own_down(c).start()

    all_ids[z] = ids[...]
    all_wts[z] = wts[...]
    tok[z] = normed[...]

    pad = size + -size % 16

    def route(d):
        @pl.when(d != z)
        def _():
            for copy in tell(d, d):
                copy.wait_recv()

        names, shares = all_ids[d], all_wts[d]
        expert = iota((pad, rows), 0) + z * size
        first, second = names[0:1, :] == expert, names[1:2, :] == expert
        hit = (first | second).astype(BF16)
        weight = jnp.where(first, shares[0:1, :], 0.0) + jnp.where(second, shares[1:2, :], 0.0)
        before = (iota((rows, rows), 0) < iota((rows, rows), 1)).astype(BF16)
        count = dot(hit, before)
        number = iota((slots, 1), 0).astype(F32)
        group = jnp.floor((number + 0.5) * (1.0 / capacity))
        place = number - group * capacity
        member = (group == iota((slots, pad), 1).astype(F32)).astype(BF16)
        chosen = (dot(member, hit) > 0.5) & (dot(member, count.astype(BF16)) == place)
        sel[d] = chosen.astype(BF16)
        comb[d] = jnp.where(chosen, dot(member, weight.astype(BF16)), 0.0).astype(BF16)

    many = len(sides) * capacity
    crowd = pl.ds(0, many)

    def dispatch(d, c, p):
        return remote(
            disp.at[slot(d, p, capacity), cols(c)], arr.at[d, block(mine), cols(c)],
            dis_s.at[d], dis_r.at[d, c], z * size + p,
        )

    def dispatched(d, c):
        at = arr.at[d, crowd, cols(c)]
        return remote(at, at, dis_s.at[d], dis_r.at[d, c], me)

    def answer(d, c, p):
        return remote(
            disp.at[slot(d, p, capacity), cols(c)], ret.at[d, block(mine), cols(c)],
            ret_s.at[d], ret_r.at[d, c], z * size + p,
        )

    def answered(d, c):
        at = ret.at[d, crowd, cols(c)]
        return remote(at, at, ret_s.at[d], ret_r.at[d, c], me)

    def partial(d, c, at, to):
        return remote(
            psend.at[row(d), cols(c)], pin.at[at, :, cols(c)],
            pin_s.at[d], pin_r.at[at, c], to,
        )

    def forward(d, c):
        @pl.when(d != z)
        def _():
            relay(d, c, me).wait_recv()

        @pl.when((d < z) & (z < planes - 1))
        def _():
            relay(d, c, me + size).start()

        @pl.when((d > z) & (z > 0))
        def _():
            relay(d, c, me - size).start()

    def lift(d, c):
        disp[slot(d), cols(c)] = dot(sel[d], tok[d, :, cols(c)]).astype(BF16)
        for p in sides:
            dispatch(d, c, p).start()

    def work(d):
        arr[d, block(mine), :] = disp[slot(d, mine, capacity), :]
        for c in range(chunks):
            dispatched(d, c).wait_recv()
        for side in range(2):

            def up(n, carry):
                at = cols(n)
                x = arr[d]
                gated = dot(x, wg[side, :, at])
                lifted = dot(x, wu[side, :, at])
                to = pl.ds(pl.multiple_of(side * part + n * tile, tile), tile)
                hidden[:, to] = (gated * jax.nn.sigmoid(gated) * lifted).astype(BF16)
                return carry

            lax.fori_loop(0, part // tile, up, 0)

    def finish(d):
        sent(disp.at[slot(d, 0, many)], dis_s.at[d]).wait_send()

        def lower(c, carry):
            disp[slot(d), cols(c)] = dot(hidden[...], wd[:, cols(c)]).astype(BF16)
            for p in sides:
                answer(d, c, p).start()
            return carry

        lax.fori_loop(0, chunks, lower, 0)
        ret[d, block(mine), :] = disp[slot(d, mine, capacity), :]

    def join(d, c):
        answered(d, c).wait_recv()
        at = cols(c)

        def own():
            return dot(comb[d], ret[d, :, at], 0, 0)

        above, below = d > z, d < z
        inner = (above & (z > 0)) | (below & (z < planes - 1))

        @pl.when(d == z)
        def _():
            acc[:, at] = acc[:, at] + own()

        @pl.when(inner)
        def _():
            partial(d, c, d, me).wait_recv()
            psend[row(d), at] = (own() + pin[d, :, at].astype(F32)).astype(BF16)

        @pl.when((d != z) & jnp.logical_not(inner))
        def _():
            psend[row(d), at] = own().astype(BF16)

        @pl.when(above)
        def _():
            partial(d, c, d, me + size).start()

        @pl.when(below)
        def _():
            partial(d, c, jnp.where(d == z - 1, planes, d), me - size).start()

    table, count = schedule(planes)

    def pick(name, step):
        found = jnp.int32(-1)
        for zz, entries in enumerate(table[name]):
            for i, value in enumerate(entries):
                if value >= 0:
                    found = jnp.where((z == zz) & (step == i), value, found)
        return found

    def turn(step, carry):
        busy, then, second = pick("work", step), pick("next", step), pick("also", step)
        mid, soon = pick("mid", step), pick("join", step)
        late, tail = pick("late", step), pick("tail", step)
        half = chunks // 2

        @pl.when(step == 1)
        def _():
            loaded()

        @pl.when(mid >= 0)
        def _():
            route(mid)
            forward(mid, 0)
            lift(mid, 0)

        @pl.when((mid >= 0) & (step == 2))
        def _():
            for c in range(1, half):
                forward(mid, c)
                lift(mid, c)

        @pl.when(busy >= 0)
        def _():
            work(busy)

        @pl.when(then >= 0)
        def _():
            route(then)
            for c in range(chunks):
                forward(then, c)

                @pl.when(second >= 0)
                def _():
                    forward(second, c)

                lift(then, c)

        @pl.when(second >= 0)
        def _():
            route(second)
            for c in range(chunks):
                lift(second, c)

        @pl.when((mid >= 0) & (step != 2))
        def _():
            for c in range(1, half):
                forward(mid, c)
                lift(mid, c)

        @pl.when((mid >= 0) & (step == 2))
        def _():
            forward(mid, half)
            lift(mid, half)

        @pl.when(busy >= 0)
        def _():
            finish(busy)

        @pl.when((mid >= 0) & (step != 2))
        def _():
            forward(mid, half)
            lift(mid, half)

        @pl.when((soon >= 0) & (step == 1))
        def _():
            join(soon, 0)

        @pl.when(mid >= 0)
        def _():
            for c in range(half + 1, chunks):
                forward(mid, c)
                lift(mid, c)

        lag = 2
        for c in range(chunks + lag):
            if c < chunks:

                @pl.when((soon >= 0) & jnp.logical_not((step == 1) & (c == 0)))
                def _():
                    join(soon, c)

            if c >= lag:

                @pl.when(tail >= 0)
                def _():
                    join(tail, c - lag)

        @pl.when(late >= 0)
        def _():
            for c in range(chunks):
                join(late, c)

        return carry

    route(z)
    for c in range(chunks):
        lift(z, c)
    lax.fori_loop(0, count, turn, 0)

    @pl.when(z < planes - 1)
    def _():
        sent(tok.at[z], tok_s.at[z]).wait_send()

    @pl.when(z > 0)
    def _():
        sent(tok.at[z], tok_s.at[planes]).wait_send()

    for c in range(chunks):
        at = cols(c)

        @pl.when(z > 0)
        def _():
            partial(z, c, z, me).wait_recv()
            acc[:, at] = acc[:, at] + pin[z, :, at].astype(F32)

        @pl.when(z < planes - 1)
        def _():
            partial(z, c, planes, me).wait_recv()
            acc[:, at] = acc[:, at] + pin[planes, :, at].astype(F32)

        out_ref[:, at] = acc[:, at].astype(BF16)

    for d in others:
        for copy in tell(d, z):
            copy.wait_send()
    def drain(d, carry):
        @pl.when(((d < z) & (z < planes - 1)) | ((d > z) & (z > 0)))
        def _():
            sent(tok.at[d], tok_s.at[d]).wait_send()

        @pl.when(d != z)
        def _():
            sent(psend.at[row(d)], pin_s.at[d]).wait_send()

        sent(disp.at[slot(d, 0, many)], ret_s.at[d]).wait_send()
        return carry

    lax.fori_loop(0, planes, drain, 0)


def layer_kernel(dims, *refs):
    planes, heads_s, heads_l, capacity, counts = dims
    refs = list(refs)

    def take(n):
        found = refs[:n]
        del refs[:n]
        return found

    given, ids, wts, own_g, own_u, own_d, out_ref = take(13), *take(6)
    wg, wu, wd, acc, disp, psend, hidden, ret = take(8)
    normed = out_ref
    lsem, xs, xr = take(3)
    mix, rest = take(counts[0]), take(counts[1])
    part, rows = own_d.shape[0], normed.shape[0]
    other = 1 - lax.axis_index("tp")
    loads = [
        pltpu.make_async_copy(src, dst, lsem.at[i])
        for i, (src, dst) in enumerate(
            ((own_g, wg.at[0]), (own_u, wu.at[0]), (own_d, wd.at[pl.ds(0, part)]))
        )
    ]
    trades = [
        pltpu.make_async_remote_copy(
            src, dst, xs.at[i], xr.at[i], device_id={"tp": other}, device_id_type=MESH
        )
        for i, (src, dst) in enumerate(
            ((own_g, wg.at[1]), (own_u, wu.at[1]), (own_d, wd.at[pl.ds(part, part)]))
        )
    ]

    def opened():
        for trade in trades[:2]:
            trade.start()
        for load in loads:
            load.start()

    def loaded():
        for load in loads:
            load.wait()
        for trade in trades:
            trade.wait_recv()

    depth = given[9].shape[0]
    mixer_part(
        (planes, heads_s, heads_l), opened, *given, acc, normed,
        disp.at[pl.ds(0, depth)], psend.at[pl.ds(0, depth)], disp.at[pl.ds(depth, rows)],
        psend.at[pl.ds(depth, rows)], ret.at[0, pl.ds(0, rows)], hidden.at[pl.ds(0, rows)], *mix,
    )
    trades[2].start()
    experts_part(
        capacity, planes, loaded, normed, ids, wts, out_ref, wg, wu, wd, acc, disp, psend, hidden, ret,
        *rest,
    )
    for trade in trades:
        trade.wait_send()


def body(*args):
    (resid, qs, ks, vs, ql, kl, vl, gs, gl, gates_s, gates_l, ws, wl, gain, ids, wts) = args[:16]
    own_w = [w[0] for w in args[16:]]
    planes = 4
    experts = args[16].shape[0] * lax.axis_size("sp")
    size = lax.axis_size("sp") // planes
    capacity = max(2, qs.shape[0] * ids.shape[1] // experts)
    capacity += -capacity % 16
    slots = size * capacity
    heads_s, heads_l = gates_s.shape[2], gates_l.shape[2]
    gates = jnp.concatenate([gates_s, gates_l], axis=2)
    gates = jnp.pad(gates, ((0, 0), (0, 0), (0, -gates.shape[2] % 8)))
    gates = jnp.transpose(gates, (1, 2, 0))
    ids, wts = ids.T, wts.T
    rows, features = resid.shape
    length = qs.shape[0]
    half = qs.shape[1] // heads_s
    pairs = qs.shape[1] // LANES
    units = pairs + heads_l
    state = pairs * half + heads_l * LANES
    part = state // size
    depth, width = own_w[0].shape
    chunks = features // 512
    vm = pl.BlockSpec(memory_space=pltpu.VMEM)
    hbm = pl.BlockSpec(memory_space=pltpu.HBM)
    vmem, dma = pltpu.VMEM, pltpu.SemaphoreType.DMA
    common = [
        vmem((2, depth, width), BF16),
        vmem((2, depth, width), BF16),
        vmem((2 * width, features), BF16),
        vmem((rows, features), F32),
        vmem((planes * slots, features), BF16),
        vmem((planes * rows, features), BF16),
        vmem((slots, 2 * width), BF16),
        vmem((planes, slots, features), BF16),
        dma((3,)),
        dma((3,)),
        dma((3,)),
    ]
    mix = [
        vmem(gs.shape, BF16),
        vmem(gl.shape, BF16),
        vmem((state, LANES), F32),
        vmem((3 * units, LANES), F32),
        vmem((state, LANES), BF16),
        vmem((size, part, LANES), BF16),
        vmem((size, 3 * units, LANES), F32),
        vmem((part, LANES), BF16),
        vmem((3 * units, LANES), F32),
        vmem((planes, part, LANES), BF16),
        vmem((planes, 3 * units, LANES), F32),
        vmem((size, part, LANES), BF16),
        vmem((state, LANES), BF16),
        vmem((3 * units, LANES), F32),
        vmem((units, length, LANES), F32),
        vmem((units, length, LANES), F32),
        vmem((units, length, LANES), F32),
        dma((5,)),
        dma((2,)),
        dma((2,)),
        dma((planes,)),
        dma((planes,)),
        dma((planes,)),
        dma((planes,)),
        dma((1,)),
        dma((1,)),
        dma((chunks,)),
        dma((chunks,)),
    ]
    rest = [
        vmem((planes,) + ids.shape, jnp.int32),
        vmem((planes,) + wts.shape, F32),
        vmem((planes, slots, rows), BF16),
        vmem((planes, slots, rows), BF16),
        vmem((planes, rows, features), BF16),
        vmem((planes, slots, features), BF16),
        vmem((planes + 1, rows, features), BF16),
        dma((planes,)),
        dma((planes,)),
        dma((planes,)),
        dma((planes,)),
        dma((planes + 1,)),
        dma((planes, chunks)),
        dma((planes,)),
        dma((planes, chunks)),
        dma((planes,)),
        dma((planes, chunks)),
        dma((planes,)),
        dma((planes + 1, chunks)),
    ]
    return pl.pallas_call(
        functools.partial(
            layer_kernel, (planes, heads_s, heads_l, capacity, (len(mix), len(rest)))
        ),
        out_shape=jax.ShapeDtypeStruct((rows, features), BF16),
        in_specs=[vm] * 7 + [hbm] * 5 + [vm] * 3 + [hbm] * 3,
        out_specs=vm,
        scratch_shapes=common + mix + rest,
        compiler_params=pltpu.CompilerParams(
            collective_id=0, has_side_effects=True, vmem_limit_bytes=67_000_000
        ),
        cost_estimate=pl.CostEstimate(
            flops=140_000_000_000, bytes_accessed=48_000_000, transcendentals=0
        ),
        name="layer",
    )(
        gates, ks, vs, kl, vl, qs, ql, gs, gl, ws, wl, resid, gain.reshape(1, -1),
        ids, wts, *own_w,
    )


def solution(mesh):
    return jax.shard_map(
        body,
        mesh=mesh,
        in_specs=(
            P(("sp", "tp"), None),
            P("sp", "tp"),
            P("sp", "tp"),
            P("sp", "tp"),
            P("sp", "tp"),
            P("sp", "tp"),
            P("sp", "tp"),
            P("sp", "tp"),
            P("sp", "tp"),
            P("sp", None, "tp"),
            P("sp", None, "tp"),
            P("tp", None),
            P("tp", None),
            P(),
            P(("sp", "tp"), None),
            P(("sp", "tp"), None),
            P("sp", None, "tp"),
            P("sp", None, "tp"),
            P("sp", "tp", None),
        ),
        out_specs=P(("sp", "tp"), None),
        check_vma=False,
    )
```

profile of v0, /device:TPU:0, one launch (start us, length us, event | category | flops | bytes accessed | tf_op | source)
XLA Modules:
  0.0 135.3 jit_solution(1379687077301490229)
XLA Ops:
  0.0 1.4 %fusion.refs_0_ = f32[3,16,384]{2,1,0:T(8,128)} fusion(f32[384,3,4]{0,2,1:T(4,128)} %param.29, f32[384,3,8]{0,2,1:T(8,128)} %param.28), kind=kLoop, calls=%fused_computation.1 | loop fusion | flops 73728 | bytes 129024 | tf_op jit(solution)/shard_map/transpose | solution.py:859
  1.4 131.8 %layer.1 = bf16[192,2048]{1,0:T(8,128)(2,1)} custom-call(f32[3,16,384]{2,1,0:T(8,128)} %fusion.refs_0_, bf16[384,512]{1,0:T(8,128)(2,1)} %refs_1_.1, bf16[384,512]{1,0:T(8,128)(2,1)} %refs_2_.1, bf16[384,512]{1,0:T(8,128)(2,1)} %refs_3_.1, bf16[384,512]{1,0:T(8,128)(2,1)} %refs_4_.1, bf16[384,512]{1,0:T(8,128)(2,1)} %refs_5_.1, bf16[384,512]{1,0:T(8,128)(2,1)} %refs_6_.1, ...), custom_call_target="tpu_custom_call" | custom-call | flops 140000002048 | bytes 48000000 | tf_op jit(solution)/shard_map/layer/pallas_call | solution.py:937
  133.2 2.1 %copy.21 = bf16[192,2048]{1,0:T(8,128)(2,1)} copy(bf16[192,2048]{1,0:T(8,128)(2,1)} %layer.1) | data formatting | bytes 1572864
where the time goes:
time: 136 us; the launch traced here: 135 us
  Pallas kernels  132 us (97%)
  local copies, waits for them, and re-layouts  2.09 us (2%)
  other arithmetic  1.43 us (1%)
    pallas_call x1, Pallas kernels, body(): pl.pallas_call(functools.partial(layer_kernel, (planes, heads_s, heads_l,...  132 us

commit v1 on v0

--- a/solution.py
+++ b/solution.py
@@ -30,10 +30,10 @@
 
 
 def mixer_part(
-    dims, opened,
-    gates, ks, vs, kl, vl, qs, ql, gs_far, gl_far, ws_far, wl_far, resid_far, gain,
+    dims, opened, leave,
+    gates, ks, vs, kl, vl, qs_far, ql_far, gs_far, gl_far, ws_far, wl_far, resid_far, gain,
     after_ref, out_ref, ws, wl, resid, psend, precv, y,
-    gs, gl,
+    qs, ql, gs, gl,
     tot_c, tot_a, give_c, got_c, got_a, sum_c, sum_a, past_c, past_a, lead_c, pre_c, pre_a,
     inum, imax, iden,
     lsem, s1, r1, s2, r2, s2a, r2a, s3, r3, psem, rsem,
@@ -55,7 +55,10 @@
     loads = [
         pltpu.make_async_copy(src, dst, lsem.at[i])
         for i, (src, dst) in enumerate(
-            ((gs_far, gs), (gl_far, gl), (ws_far, ws), (wl_far, wl), (resid_far, resid))
+            (
+                (qs_far, qs), (ql_far, ql), (gs_far, gs), (gl_far, gl),
+                (ws_far, ws), (wl_far, wl), (resid_far, resid),
+            )
         )
     ]
     for load in loads:
@@ -234,6 +237,8 @@
         for copy in first(p):
             copy.start()
     opened()
+    for load in loads[:2]:
+        load.wait()
     for unit in range(pairs):
         inner(unit)
     for copy in firsts:
@@ -292,7 +297,7 @@
         if j < size - 1:
             ew, lw = wide[planes + 2 * j : planes + 2 * j + 2]
             state_c = ew * state_c + lw * got_c[j].astype(F32)
-    for load in loads:
+    for load in loads[2:]:
         load.wait()
     thirds.wait_recv()
 
@@ -370,6 +375,7 @@
     for n in range(0, features, step_n):
         at = (slice(None), slice(n, n + step_n))
         out_ref[at] = (after_ref[at] * scale * gain[:, n : n + step_n]).astype(BF16)
+        leave(n // step_n)
 
     for copy in firsts:
         copy.wait_send()
@@ -471,18 +477,6 @@
             remote(wts, all_wts.at[at], wts_s.at[d], wts_r.at[at], to),
         )
 
-    def own_up(c):
-        return remote(
-            normed.at[:, cols(c)], tok.at[z, :, cols(c)], tok_s.at[z], tok_r.at[z, c],
-            me + size,
-        )
-
-    def own_down(c):
-        return remote(
-            normed.at[:, cols(c)], tok.at[z, :, cols(c)], tok_s.at[planes], tok_r.at[z, c],
-            me - size,
-        )
-
     def relay(d, c, to):
         return remote(
             tok.at[d, :, cols(c)], tok.at[d, :, cols(c)], tok_s.at[d], tok_r.at[d, c], to
@@ -491,16 +485,6 @@
     for d in others:
         for copy in tell(d, z):
             copy.start()
-    for c in range(chunks):
-
-        @pl.when(z < planes - 1)
-        def _():
-            own_up(c).start()
-
-        @pl.when(z > 0)
-        def _():
-            own_down(c).start()
-
     all_ids[z] = ids[...]
     all_wts[z] = wts[...]
     tok[z] = normed[...]
@@ -829,9 +813,31 @@
         for trade in trades:
             trade.wait_recv()
 
+    tok, tok_s, tok_r = rest[4], rest[11], rest[12]
+    me = lax.axis_index("sp")
+    size = lax.axis_size("sp") // planes
+    z = me // size
+
+    def leave(c):
+        at = (slice(None), pl.ds(c * 512, 512))
+
+        def go(to, sem):
+            pltpu.make_async_remote_copy(
+                normed.at[at], tok.at[z].at[at], sem, tok_r.at[z, c],
+                device_id={"sp": to}, device_id_type=MESH,
+            ).start()
+
+        @pl.when(z < planes - 1)
+        def _():
+            go(me + size, tok_s.at[z])
+
+        @pl.when(z > 0)
+        def _():
+            go(me - size, tok_s.at[planes])
+
     depth = given[9].shape[0]
     mixer_part(
-        (planes, heads_s, heads_l), opened, *given, acc, normed,
+        (planes, heads_s, heads_l), opened, leave, *given, acc, normed,
         disp.at[pl.ds(0, depth)], psend.at[pl.ds(0, depth)], disp.at[pl.ds(depth, rows)],
         psend.at[pl.ds(depth, rows)], ret.at[0, pl.ds(0, rows)], hidden.at[pl.ds(0, rows)], *mix,
     )
@@ -884,6 +890,8 @@
         dma((3,)),
     ]
     mix = [
+        vmem(qs.shape, BF16),
+        vmem(ql.shape, BF16),
         vmem(gs.shape, BF16),
         vmem(gl.shape, BF16),
         vmem((state, LANES), F32),
@@ -901,7 +909,7 @@
         vmem((units, length, LANES), F32),
         vmem((units, length, LANES), F32),
         vmem((units, length, LANES), F32),
-        dma((5,)),
+        dma((7,)),
         dma((2,)),
         dma((2,)),
         dma((planes,)),
@@ -939,7 +947,7 @@
             layer_kernel, (planes, heads_s, heads_l, capacity, (len(mix), len(rest)))
         ),
         out_shape=jax.ShapeDtypeStruct((rows, features), BF16),
-        in_specs=[vm] * 7 + [hbm] * 5 + [vm] * 3 + [hbm] * 3,
+        in_specs=[vm] * 5 + [hbm] * 7 + [vm] * 3 + [hbm] * 3,
         out_specs=vm,
         scratch_shapes=common + mix + rest,
         compiler_params=pltpu.CompilerParams(

time: 136 us -> 139 us (1.022)
  Pallas kernels: 132 us -> 136 us
    pallas_call x1, Pallas kernels: 132 us -> 136 us  [body(): pl.pallas_call(functools.partial(layer_kernel, (planes, heads_s, heads_l,...]
where the time goes in v1:
time: 139 us
  Pallas kernels  136 us (98%)
  local copies, waits for them, and re-layouts  2.09 us (2%)
  other arithmetic  1.43 us (1%)
    pallas_call x1, Pallas kernels, body(): pl.pallas_call(functools.partial(layer_kernel, (planes, heads_s, heads_l,...  136 us

profile of v1, /device:TPU:0, one launch (start us, length us, event | category | flops | bytes accessed | tf_op | source)
XLA Modules:
  0.0 139.2 jit_solution(9450965406504995104)
XLA Ops:
  0.0 1.4 %fusion.refs_0_ = f32[3,16,384]{2,1,0:T(8,128)} fusion(f32[384,3,4]{0,2,1:T(4,128)} %param.29, f32[384,3,8]{0,2,1:T(8,128)} %param.28), kind=kLoop, calls=%fused_computation.1 | loop fusion | flops 73728 | bytes 129024 | tf_op jit(solution)/shard_map/transpose | solution.py:865
  1.4 135.6 %layer.1 = bf16[192,2048]{1,0:T(8,128)(2,1)} custom-call(f32[3,16,384]{2,1,0:T(8,128)} %fusion.refs_0_, bf16[384,512]{1,0:T(8,128)(2,1)} %refs_1_.1, bf16[384,512]{1,0:T(8,128)(2,1)} %refs_2_.1, bf16[384,512]{1,0:T(8,128)(2,1)} %refs_3_.1, bf16[384,512]{1,0:T(8,128)(2,1)} %refs_4_.1, bf16[384,512]{1,0:T(8,128)(2,1)} %refs_5_.1, bf16[384,512]{1,0:T(8,128)(2,1)} %refs_6_.1, ...), custom_call_target="tpu_custom_call" | custom-call | flops 140000002048 | bytes 48000000 | tf_op jit(solution)/shard_map/layer/pallas_call | solution.py:945
  137.1 2.1 %copy.21 = bf16[192,2048]{1,0:T(8,128)(2,1)} copy(bf16[192,2048]{1,0:T(8,128)(2,1)} %layer.1) | data formatting | bytes 1572864
